TPU v7x, 32 devices: a whole 2x2x4 slice. The times are simulated.
32 devices in a mesh: ra: 4 (over z), cb: 4 (over y, x), dp: 2 (over core).
Axes of the slice: x: 2, y: 2, z: 4, core: 2. Of those that a mesh axis runs over, the one named last changes fastest.
Arguments:
- tokens: bfloat16 [256, 2048], P('dp', 'ra'), may hold values from -200 to 200, as said below
- first_gain: float32 [2048], P('ra'), may hold values from 0.1 to 1.9
- first_gate: float32 [2048, 5632], P('ra', 'cb'), may hold values from -0.125 to 0.125
- first_gate_scale: float32 [5632], P('cb'), may hold values from 0.5 to 2
- first_up: float32 [2048, 5632], P('ra', 'cb'), may hold values from -0.125 to 0.125
- first_up_scale: float32 [5632], P('cb'), may hold values from 0.5 to 2
- first_down: float32 [5632, 2048], P('cb', 'ra'), may hold values from -0.078125 to 0.078125
- first_down_scale: float32 [2048], P('ra'), may hold values from 0.5 to 2
- second_gain: float32 [2048], P('ra'), may hold values from 0.1 to 1.9
- second_gate: float32 [2048, 5632], P('ra', 'cb'), may hold values from -0.125 to 0.125
- second_gate_scale: float32 [5632], P('cb'), may hold values from 0.5 to 2
- second_up: float32 [2048, 5632], P('ra', 'cb'), may hold values from -0.125 to 0.125
- second_up_scale: float32 [5632], P('cb'), may hold values from 0.5 to 2
- second_down: float32 [5632, 2048], P('cb', 'ra'), may hold values from -0.078125 to 0.078125
- second_down_scale: float32 [2048], P('ra'), may hold values from 0.5 to 2
Outputs:
- stream_out: bfloat16 [256, 2048], P('dp', 'ra')
Inputs may be any that keep to these rules, and one draw needn't show every extreme that they name: `tokens`: Per-token and per-feature magnitudes vary.
All inputs are finite; a program needn't handle non-finite values.
Results may differ from a plain program's by a relative error of at most 0.039.
Values may be sent and summed in bfloat16 or wider, within the bound.
A program may use at most 64 MiB of HBM per device.

v0:
```python
import jax
import jax.numpy as jnp
from jax import lax
from jax.sharding import PartitionSpec as P

D = 2048
EPS = 1e-06
RESID = 0.5


def sublayer(stream, gain, w_gate, gate_scale, w_up, up_scale, w_down, down_scale):
    values = stream.astype(jnp.float32)
    sum_sq = lax.psum(jnp.sum(values * values, -1), "ra")
    normed = (values * lax.rsqrt(sum_sq / D + EPS)[:, None] * gain).astype(jnp.bfloat16)
    part_gate = jnp.dot(normed, w_gate.astype(jnp.bfloat16), preferred_element_type=jnp.float32)
    part_up = jnp.dot(normed, w_up.astype(jnp.bfloat16), preferred_element_type=jnp.float32)
    gate, up = (
        lax.psum(part_gate.astype(jnp.bfloat16), "ra").astype(jnp.float32),
        lax.psum(part_up.astype(jnp.bfloat16), "ra").astype(jnp.float32),
    )
    hidden = (jax.nn.silu(gate * gate_scale) * (up * up_scale)).astype(jnp.bfloat16)
    partial_value = jnp.dot(hidden, w_down.astype(jnp.bfloat16), preferred_element_type=jnp.float32)
    branch = lax.psum(partial_value.astype(jnp.bfloat16), "cb").astype(jnp.float32)
    return (RESID * values + branch * down_scale).astype(jnp.bfloat16)


def body(
    tokens,
    first_gain,
    first_gate,
    first_gate_scale,
    first_up,
    first_up_scale,
    first_down,
    first_down_scale,
    second_gain,
    second_gate,
    second_gate_scale,
    second_up,
    second_up_scale,
    second_down,
    second_down_scale,
):
    middle = sublayer(
        tokens,
        first_gain,
        first_gate,
        first_gate_scale,
        first_up,
        first_up_scale,
        first_down,
        first_down_scale,
    )
    return sublayer(
        middle,
        second_gain,
        second_gate,
        second_gate_scale,
        second_up,
        second_up_scale,
        second_down,
        second_down_scale,
    )


def solution(mesh):
    in_specs = (
        P("dp", "ra"),
        P("ra"),
        P("ra", "cb"),
        P("cb"),
        P("ra", "cb"),
        P("cb"),
        P("cb", "ra"),
        P("ra"),
        P("ra"),
        P("ra", "cb"),
        P("cb"),
        P("ra", "cb"),
        P("cb"),
        P("cb", "ra"),
        P("ra"),
    )
    out_specs = P("dp", "ra")
    return jax.shard_map(body, mesh=mesh, in_specs=in_specs, out_specs=out_specs, check_vma=False)
```

profile of v0, /device:TPU:0, one launch (start us, length us, event | category | flops | bytes accessed | tf_op | source)
XLA Modules:
  0.0 218.9 jit_solution(4206691932930138170)
XLA Ops:
  6.5 1.2 fusion.22
  7.7 13.5 %psum.56 = f32[128]{0:T(128)S(1)} all-reduce(f32[128]{0:T(128)S(1)} %fusion.22), channel_id=1, replica_groups=mesh['ra'=4,'cb'=4,'dp'=2] {'ra'}, use_global_device_ids=true, to_apply=%region_1.0 | all-reduce | flops 128 | bytes 1024 | tf_op jit(solution)/shard_map/psum | solution.py:13
  21.2 3.1 %convolution_convert_fusion.2 = bf16[128,1408]{1,0:T(8,128)(2,1)} fusion(f32[512,1408]{1,0:T(8,128)} %param.19, bf16[128,512]{1,0:T(8,128)(2,1)} %param.15, f32[512]{0:T(512)} %param.16, f32[128]{0:T(128)S(1)} %add_rsqrt_fusion.1), kind=kOutput, calls=%fused_computation.2 | convolution fusion | flops 185712640 | bytes 3377664 | tf_op jit(solution)/shard_map/dot_general | solution.py:16
  24.3 0.0 copy-start.9
  24.3 1.2 convolution_convert_fusion.3
  25.5 0.0 all-reduce.13.cloned.1.call-update
  25.5 0.0 all-reduce.7.cloned.1.call-start
  25.6 40.3 %all-reduce.13.cloned.1.call-done = (bf16[128,1408]{1,0:T(8,128)(2,1)}, bf16[128,1408]{1,0:T(8,128)(2,1)}) async-done(((bf16[128,1408]{1,0:T(8,128)(2,1)}, bf16[128,1408]{1,0:T(8,128)(2,1)}), (bf16[128,1408]{1,0:T(8,128)(2,1)}, bf16[128,1408]{1,0:T(8,128)(2,1)})) %all-reduce.13.cloned.1.call-update) | async-done | bytes 720912 | tf_op jit(solution)/shard_map/psum | solution.py:19
  65.9 3.2 %fusion.8 = bf16[128,512]{1,0:T(8,128)(2,1)} fusion(f32[1408,512]{1,0:T(8,128)} %param.21, bf16[128,1408]{1,0:T(8,128)(2,1)} %get-tuple-element.7, bf16[128,1408]{1,0:T(8,128)(2,1)} %get-tuple-element.8, f32[1408]{0:T(1024)S(1)} %copy-done.9, f32[1408]{0:T(1024)S(1)} %copy-done.10), kind=kOutput, calls=%fused_computation.12 | convolution fusion | flops 187138048 | bytes 3746816 | tf_op jit(solution)/shard_map/dot_general | solution.py:22
  69.1 0.0 all-reduce.7.cloned.1.call-update
  69.1 0.0 all-reduce.11.cloned.1.call-start
  69.1 41.8 %all-reduce.7.cloned.1.call-done = bf16[128,512]{1,0:T(8,128)(2,1)} async-done(((bf16[128,512]{1,0:T(8,128)(2,1)}), bf16[128,512]{1,0:T(8,128)(2,1)}) %all-reduce.7.cloned.1.call-update) | async-done | bytes 131088 | tf_op jit(solution)/shard_map/psum | solution.py:23
  111.0 1.0 fusion.27
  112.0 11.7 %psum.60 = f32[128]{0:T(128)S(1)} all-reduce(f32[128]{0:T(128)S(1)} %get-tuple-element.9), channel_id=1, replica_groups=mesh['ra'=4,'cb'=4,'dp'=2] {'ra'}, use_global_device_ids=true, to_apply=%region_6.7 | all-reduce | flops 128 | bytes 1024 | tf_op jit(solution)/shard_map/psum | solution.py:13
  123.7 1.2 convolution_convert_fusion
  124.9 0.8 copy-done.2
  125.7 1.2 convolution_convert_fusion.1
  126.8 0.0 all-reduce.11.cloned.1.call-update
  126.9 0.0 all-reduce.9.cloned.1.call-start
  126.9 39.3 %all-reduce.11.cloned.1.call-done = (bf16[128,1408]{1,0:T(8,128)(2,1)}, bf16[128,1408]{1,0:T(8,128)(2,1)}) async-done(((bf16[128,1408]{1,0:T(8,128)(2,1)}, bf16[128,1408]{1,0:T(8,128)(2,1)}), (bf16[128,1408]{1,0:T(8,128)(2,1)}, bf16[128,1408]{1,0:T(8,128)(2,1)})) %all-reduce.11.cloned.1.call-update) | async-done | bytes 720912 | tf_op jit(solution)/shard_map/psum | solution.py:19
  166.3 2.3 %fusion.11 = bf16[128,512]{1,0:T(8,128)(2,1)} fusion(f32[1408,512]{1,0:T(8,128)S(1)} %copy-done.8, bf16[128,1408]{1,0:T(8,128)(2,1)} %get-tuple-element.5, bf16[128,1408]{1,0:T(8,128)(2,1)} %get-tuple-element.6, f32[1408]{0:T(1024)S(1)} %copy-done.11, f32[1408]{0:T(1024)S(1)} %copy-done.12), kind=kOutput, calls=%fused_computation.13 | convolution fusion | flops 187138048 | bytes 3746816 | tf_op jit(solution)/shard_map/dot_general | solution.py:22
  168.5 0.0 all-reduce.9.cloned.1.call-update
  168.6 42.2 %all-reduce.9.cloned.1.call-done = bf16[128,512]{1,0:T(8,128)(2,1)} async-done(((bf16[128,512]{1,0:T(8,128)(2,1)}), bf16[128,512]{1,0:T(8,128)(2,1)}) %all-reduce.9.cloned.1.call-update) | async-done | bytes 131088 | tf_op jit(solution)/shard_map/psum | solution.py:23
  210.8 1.6 fusion.26
  (27 shorter events, 0.1 us)
Async XLA Ops:
  6.5 17.7 %copy-start.3 = (bf16[128,512]{1,0:T(8,128)(2,1)S(1)}, bf16[128,512]{1,0:T(8,128)(2,1)}, u32[]{:S(2)}) copy-start(bf16[128,512]{1,0:T(8,128)(2,1)} %param.15) | copy-start | bytes 393220
  6.5 17.7 %copy-start.4 = (f32[512]{0:T(512)S(1)}, f32[512]{0:T(512)}, u32[]{:S(2)}) copy-start(f32[512]{0:T(512)} %param.16) | copy-start | bytes 6148
  6.5 17.7 %copy-start = (f32[512,1408]{1,0:T(8,128)S(1)}, f32[512,1408]{1,0:T(8,128)}, u32[]{:S(2)}) copy-start(f32[512,1408]{1,0:T(8,128)} %param.17) | copy-start | bytes 8650756
  6.5 59.3 %all-reduce.13.cloned.1.call-start = ((), (), s32[]{:S(2)}) async-start(), calls=%async_computation.3 | async-start | bytes 1441792 | tf_op jit(solution)/shard_map/psum | solution.py:19
  24.3 41.6 %copy-start.9 = (f32[1408]{0:T(1024)S(1)}, f32[1408]{0:T(1024)}, u32[]{:S(2)}) copy-start(f32[1408]{0:T(1024)} %param.20) | copy-start | bytes 16900
  24.3 41.6 %copy-start.10 = (f32[1408]{0:T(1024)S(1)}, f32[1408]{0:T(1024)}, u32[]{:S(2)}) copy-start(f32[1408]{0:T(1024)} %param.18) | copy-start | bytes 16900
  25.5 85.5 %copy-start.6 = (f32[512]{0:T(512)S(1)}, f32[512]{0:T(512)}, u32[]{:S(2)}) copy-start(f32[512]{0:T(512)} %param.22) | copy-start | bytes 6148
  25.5 98.2 %copy-start.1 = (f32[512,1408]{1,0:T(8,128)S(1)}, f32[512,1408]{1,0:T(8,128)}, u32[]{:S(2)}) copy-start(f32[512,1408]{1,0:T(8,128)} %param.26) | copy-start | bytes 8650756
  25.5 98.2 %copy-start.5 = (f32[512]{0:T(512)S(1)}, f32[512]{0:T(512)}, u32[]{:S(2)}) copy-start(f32[512]{0:T(512)} %param.23) | copy-start | bytes 6148
  25.5 85.5 %all-reduce.7.cloned.1.call-start = ((), (), s32[]{:S(2)}) async-start(), calls=%async_computation | async-start | bytes 262144 | tf_op jit(solution)/shard_map/psum | solution.py:23
  69.1 97.2 %all-reduce.11.cloned.1.call-start = ((), (), s32[]{:S(2)}) async-start(), calls=%async_computation.2 | async-start | bytes 1441792 | tf_op jit(solution)/shard_map/psum | solution.py:19
  123.7 1.9 copy-start.2
  125.7 40.6 %copy-start.8 = (f32[1408,512]{1,0:T(8,128)S(1)}, f32[1408,512]{1,0:T(8,128)}, u32[]{:S(2)}) copy-start(f32[1408,512]{1,0:T(8,128)} %param.28) | copy-start | bytes 8650756
  125.7 40.6 %copy-start.11 = (f32[1408]{0:T(1024)S(1)}, f32[1408]{0:T(1024)}, u32[]{:S(2)}) copy-start(f32[1408]{0:T(1024)} %param.27) | copy-start | bytes 16900
  125.7 40.6 %copy-start.12 = (f32[1408]{0:T(1024)S(1)}, f32[1408]{0:T(1024)}, u32[]{:S(2)}) copy-start(f32[1408]{0:T(1024)} %param.25) | copy-start | bytes 16900
  126.8 83.9 %copy-start.7 = (f32[512]{0:T(512)S(1)}, f32[512]{0:T(512)}, u32[]{:S(2)}) copy-start(f32[512]{0:T(512)} %param.29) | copy-start | bytes 6148
  126.9 83.9 %all-reduce.9.cloned.1.call-start = ((), (), s32[]{:S(2)}) async-start(), calls=%async_computation.1 | async-start | bytes 262144 | tf_op jit(solution)/shard_map/psum | solution.py:23
Sparse Core Ops, SparseCore 0:
  25.6 40.1 all-reduce.12
  69.2 41.7 all-reduce.6
  127.0 39.2 all-reduce.10
  169.0 41.7 all-reduce.8
where the time goes:
time: 219 us
  waiting for transfers between devices  164 us (75%)
  blocking collectives  25.2 us (12%)
  between operations  13.2 us (6%)
  matrix products  12 us (5%)
  other arithmetic  3.83 us (2%)
    psum x2, waiting for transfers between devices, sublayer(): lax.psum(partial_value.astype(jnp.bfloat16), 'cb').astype(jnp.float32)  84 us
    psum x2, waiting for transfers between devices, sublayer(): lax.psum(part_up.astype(jnp.bfloat16), 'ra').astype(jnp.float32)  79.7 us
    psum x2, blocking collectives, sublayer(): sum_sq = lax.psum(jnp.sum(values * values, -1), 'ra')  25.2 us
    dot_general x2, matrix products, sublayer(): jnp.dot(hidden, w_down.astype(jnp.bfloat16), preferred_element_type=jnp.f...  5.45 us
  transfers between devices with their start and end apart: 4, of which 4 were waited for; matrix products, arithmetic and copies ran while one was open for 0% of the time, Pallas kernels for 0%

commit v1 on v0

--- a/solution.py
+++ b/solution.py
@@ -8,6 +8,12 @@
 RESID = 0.5
 
 
+def gather_and_add(x, axis):
+    pieces = lax.all_gather(x, axis, axis=0, tiled=False)
+    total = pieces.sum(axis=0)
+    return total
+
+
 def sublayer(stream, gain, w_gate, gate_scale, w_up, up_scale, w_down, down_scale):
     values = stream.astype(jnp.float32)
     sum_sq = lax.psum(jnp.sum(values * values, -1), "ra")
@@ -16,7 +22,7 @@
     part_up = jnp.dot(normed, w_up.astype(jnp.bfloat16), preferred_element_type=jnp.float32)
     gate, up = (
         lax.psum(part_gate.astype(jnp.bfloat16), "ra").astype(jnp.float32),
-        lax.psum(part_up.astype(jnp.bfloat16), "ra").astype(jnp.float32),
+        gather_and_add(part_up.astype(jnp.bfloat16), "ra").astype(jnp.float32),
     )
     hidden = (jax.nn.silu(gate * gate_scale) * (up * up_scale)).astype(jnp.bfloat16)
     partial_value = jnp.dot(hidden, w_down.astype(jnp.bfloat16), preferred_element_type=jnp.float32)

time: 219 us -> 278 us (1.27)
  waiting for transfers between devices: 164 us -> 218 us
  other arithmetic: 3.83 us -> 7.05 us
    all_gather x0 -> x2, waiting for transfers between devices: none -> 60.7 us  [gather_and_add(): pieces = lax.all_gather(x, axis, axis=0, tiled=False)]
    psum x2, waiting for transfers between devices: 79.7 us -> 72.3 us  [sublayer(): lax.psum(part_gate.astype(jnp.bfloat16), 'ra').astype(jnp.float32)]
    reduce_sum x0 -> x2, other arithmetic: none -> 3.21 us  [gather_and_add(): total = pieces.sum(axis=0)]
  transfers between devices with their start and end apart: 4 -> 6, of which waited for: 4 -> 6; matrix products, arithmetic and copies ran while one was open for 0% -> 3% of each run, Pallas kernels for 0% -> 0%
where the time goes in v1:
time: 278 us
  waiting for transfers between devices  218 us (78%)
  blocking collectives  25.2 us (9%)
  matrix products  13.7 us (5%)
  between operations  13.5 us (5%)
  other arithmetic  7.05 us (3%)
    psum x2, waiting for transfers between devices, sublayer(): lax.psum(partial_value.astype(jnp.bfloat16), 'cb').astype(jnp.float32)  84.7 us
    psum x2, waiting for transfers between devices, sublayer(): lax.psum(part_gate.astype(jnp.bfloat16), 'ra').astype(jnp.float32)  72.3 us
    all_gather x2, waiting for transfers between devices, gather_and_add(): pieces = lax.all_gather(x, axis, axis=0, tiled=False)  60.7 us
    psum x2, blocking collectives, sublayer(): sum_sq = lax.psum(jnp.sum(values * values, -1), 'ra')  25.2 us
  transfers between devices with their start and end apart: 6, of which 6 were waited for; matrix products, arithmetic and copies ran while one was open for 3% of the time, Pallas kernels for 0%

profile of v1, /device:TPU:0, one launch (start us, length us, event | category | flops | bytes accessed | tf_op | source)
XLA Modules:
  0.0 277.6 jit_solution(10535501963997082981)
XLA Ops:
  6.5 1.2 fusion.22
  7.7 13.5 %psum.42 = f32[128]{0:T(128)S(1)} all-reduce(f32[128]{0:T(128)S(1)} %fusion.22), channel_id=1, replica_groups=mesh['ra'=4,'cb'=4,'dp'=2] {'ra'}, use_global_device_ids=true, to_apply=%region_1.0 | all-reduce | flops 128 | bytes 1024 | tf_op jit(solution)/shard_map/psum | solution.py:19
  21.2 3.1 %convolution_convert_fusion.2 = bf16[128,1408]{1,0:T(8,128)(2,1)} fusion(f32[512,1408]{1,0:T(8,128)} %param.19, bf16[128,512]{1,0:T(8,128)(2,1)} %param.15, f32[512]{0:T(512)} %param.16, f32[128]{0:T(128)S(1)} %add_rsqrt_fusion.1), kind=kOutput, calls=%fused_computation.2 | convolution fusion | flops 185712640 | bytes 3377664 | tf_op jit(solution)/shard_map/dot_general | solution.py:22
  24.3 0.0 all-reduce.5.cloned.1.call-start
  24.4 1.2 convolution_convert_fusion.3
  25.6 0.0 all-reduce.7.cloned.1.call-start
  25.6 31.8 %all-gather.5.cloned.1.call-done = bf16[512,1408]{1,0:T(8,128)(2,1)} async-done(((bf16[128,1408]{1,0:T(8,128)(2,1)}), bf16[512,1408]{1,0:T(8,128)(2,1)}) %all-gather.5.cloned.1.call-update) | async-done | bytes 1441808 | tf_op jit(solution)/shard_map/all_gather | solution.py:12
  57.4 1.6 reduce_sum.43
  59.1 36.2 %all-reduce.5.cloned.1.call-done = bf16[128,1408]{1,0:T(8,128)(2,1)} async-done(((bf16[128,1408]{1,0:T(8,128)(2,1)}), bf16[128,1408]{1,0:T(8,128)(2,1)}) %all-reduce.5.cloned.1.call-update) | async-done | bytes 360464 | tf_op jit(solution)/shard_map/psum | solution.py:24
  95.3 3.1 %fusion.8 = bf16[128,512]{1,0:T(8,128)(2,1)} fusion(f32[1408,512]{1,0:T(8,128)} %param.21, bf16[128,1408]{1,0:T(8,128)(2,1)S(1)} %reduce_sum.43, bf16[128,1408]{1,0:T(8,128)(2,1)} %all-reduce.5.cloned.1.call-done, f32[1408]{0:T(1024)S(1)} %copy-done.8, f32[1408]{0:T(1024)S(1)} %copy-done.9), kind=kOutput, calls=%fused_computation.12 | convolution fusion | flops 187138048 | bytes 3746816 | tf_op jit(solution)/shard_map/dot_general | solution.py:28
  98.4 0.0 all-gather.7.cloned.1.call-start
  98.5 42.1 %all-reduce.7.cloned.1.call-done = bf16[128,512]{1,0:T(8,128)(2,1)} async-done(((bf16[128,512]{1,0:T(8,128)(2,1)}), bf16[128,512]{1,0:T(8,128)(2,1)}) %all-reduce.7.cloned.1.call-update) | async-done | bytes 131088 | tf_op jit(solution)/shard_map/psum | solution.py:29
  140.6 1.0 fusion.27
  141.6 11.7 %psum.45 = f32[128]{0:T(128)S(1)} all-reduce(f32[128]{0:T(128)S(1)} %get-tuple-element.5), channel_id=1, replica_groups=mesh['ra'=4,'cb'=4,'dp'=2] {'ra'}, use_global_device_ids=true, to_apply=%region_6.7 | all-reduce | flops 128 | bytes 1024 | tf_op jit(solution)/shard_map/psum | solution.py:19
  153.3 1.2 convolution_convert_fusion
  154.5 0.0 all-reduce.9.cloned.1.call-start
  154.6 3.1 %convolution_convert_fusion.1 = bf16[128,1408]{1,0:T(8,128)(2,1)} fusion(f32[512,1408]{1,0:T(8,128)} %param.24, bf16[128,512]{1,0:T(8,128)(2,1)S(1)} %get-tuple-element.6, f32[512]{0:T(512)S(1)} %copy-done.4, f32[128]{0:T(128)S(1)} %add_rsqrt_fusion), kind=kOutput, calls=%fused_computation.1 | convolution fusion | flops 185712640 | bytes 3377664 | tf_op jit(solution)/shard_map/dot_general | solution.py:21
  157.7 0.0 all-reduce.11.cloned.1.call-start
  157.8 28.9 %all-gather.7.cloned.1.call-done = bf16[512,1408]{1,0:T(8,128)(2,1)} async-done(((bf16[128,1408]{1,0:T(8,128)(2,1)}), bf16[512,1408]{1,0:T(8,128)(2,1)}) %all-gather.7.cloned.1.call-update) | async-done | bytes 1441808 | tf_op jit(solution)/shard_map/all_gather | solution.py:12
  186.7 1.6 reduce_sum.45
  188.3 36.1 %all-reduce.9.cloned.1.call-done = bf16[128,1408]{1,0:T(8,128)(2,1)} async-done(((bf16[128,1408]{1,0:T(8,128)(2,1)}), bf16[128,1408]{1,0:T(8,128)(2,1)}) %all-reduce.9.cloned.1.call-update) | async-done | bytes 360464 | tf_op jit(solution)/shard_map/psum | solution.py:24
  224.4 2.1 fusion.11
  226.6 42.6 %all-reduce.11.cloned.1.call-done = bf16[128,512]{1,0:T(8,128)(2,1)} async-done(((bf16[128,512]{1,0:T(8,128)(2,1)}), bf16[128,512]{1,0:T(8,128)(2,1)}) %all-reduce.11.cloned.1.call-update) | async-done | bytes 131088 | tf_op jit(solution)/shard_map/psum | solution.py:29
  269.2 1.6 fusion.26
  (33 shorter events, 0.2 us)
Async XLA Ops:
  6.5 17.8 %copy-start.2 = (bf16[128,512]{1,0:T(8,128)(2,1)S(1)}, bf16[128,512]{1,0:T(8,128)(2,1)}, u32[]{:S(2)}) copy-start(bf16[128,512]{1,0:T(8,128)(2,1)} %param.15) | copy-start | bytes 393220
  6.5 17.8 %copy-start.3 = (f32[512]{0:T(512)S(1)}, f32[512]{0:T(512)}, u32[]{:S(2)}) copy-start(f32[512]{0:T(512)} %param.16) | copy-start | bytes 6148
  6.5 17.8 %copy-start = (f32[512,1408]{1,0:T(8,128)S(1)}, f32[512,1408]{1,0:T(8,128)}, u32[]{:S(2)}) copy-start(f32[512,1408]{1,0:T(8,128)} %param.17) | copy-start | bytes 8650756
  6.5 50.9 %all-gather.5.cloned.1.call-start = ((), (), s32[]{:S(2)}) async-start(), calls=%async_computation.4 | async-start | bytes 1802240 | tf_op jit(solution)/shard_map/all_gather | solution.py:12
  24.3 71.0 %copy-start.8 = (f32[1408]{0:T(1024)S(1)}, f32[1408]{0:T(1024)}, u32[]{:S(2)}) copy-start(f32[1408]{0:T(1024)} %param.20) | copy-start | bytes 16900
  24.3 71.0 %copy-start.9 = (f32[1408]{0:T(1024)S(1)}, f32[1408]{0:T(1024)}, u32[]{:S(2)}) copy-start(f32[1408]{0:T(1024)} %param.18) | copy-start | bytes 16900
  24.3 71.0 %all-reduce.5.cloned.1.call-start = ((), (), s32[]{:S(2)}) async-start(), calls=%async_computation | async-start | bytes 720896 | tf_op jit(solution)/shard_map/psum | solution.py:24
  25.6 115.0 %all-reduce.7.cloned.1.call-start = ((), (), s32[]{:S(2)}) async-start(), calls=%async_computation.1 | async-start | bytes 262144 | tf_op jit(solution)/shard_map/psum | solution.py:29
  57.4 83.2 %copy-start.5 = (f32[512]{0:T(512)S(1)}, f32[512]{0:T(512)}, u32[]{:S(2)}) copy-start(f32[512]{0:T(512)} %param.22) | copy-start | bytes 6148
  59.0 94.3 %copy-start.1 = (f32[512,1408]{1,0:T(8,128)S(1)}, f32[512,1408]{1,0:T(8,128)}, u32[]{:S(2)}) copy-start(f32[512,1408]{1,0:T(8,128)} %param.26) | copy-start | bytes 8650756
  59.1 94.3 %copy-start.4 = (f32[512]{0:T(512)S(1)}, f32[512]{0:T(512)}, u32[]{:S(2)}) copy-start(f32[512]{0:T(512)} %param.23) | copy-start | bytes 6148
  98.4 88.3 %all-gather.7.cloned.1.call-start = ((), (), s32[]{:S(2)}) async-start(), calls=%async_computation.5 | async-start | bytes 1802240 | tf_op jit(solution)/shard_map/all_gather | solution.py:12
  154.5 69.9 %copy-start.7 = (f32[1408,512]{1,0:T(8,128)S(1)}, f32[1408,512]{1,0:T(8,128)}, u32[]{:S(2)}) copy-start(f32[1408,512]{1,0:T(8,128)} %param.28) | copy-start | bytes 8650756
  154.5 69.9 %copy-start.10 = (f32[1408]{0:T(1024)S(1)}, f32[1408]{0:T(1024)}, u32[]{:S(2)}) copy-start(f32[1408]{0:T(1024)} %param.27) | copy-start | bytes 16900
  154.5 69.9 %copy-start.11 = (f32[1408]{0:T(1024)S(1)}, f32[1408]{0:T(1024)}, u32[]{:S(2)}) copy-start(f32[1408]{0:T(1024)} %param.25) | copy-start | bytes 16900
  154.5 69.9 %all-reduce.9.cloned.1.call-start = ((), (), s32[]{:S(2)}) async-start(), calls=%async_computation.2 | async-start | bytes 720896 | tf_op jit(solution)/shard_map/psum | solution.py:24
  157.7 111.5 %all-reduce.11.cloned.1.call-start = ((), (), s32[]{:S(2)}) async-start(), calls=%async_computation.3 | async-start | bytes 262144 | tf_op jit(solution)/shard_map/psum | solution.py:29
  186.7 82.5 %copy-start.6 = (f32[512]{0:T(512)S(1)}, f32[512]{0:T(512)}, u32[]{:S(2)}) copy-start(f32[512]{0:T(512)} %param.29) | copy-start | bytes 6148
Sparse Core Ops, SparseCore 0:
  24.4 32.9 all-gather.4
  59.8 35.4 all-reduce.4
  98.6 41.9 all-reduce.6
  154.7 31.9 all-gather.6
  188.9 35.4 all-reduce.8
  227.2 41.9 all-reduce.10
